TPU v7x, 128 devices: a whole 4x4x4 slice. The times are simulated.
128 devices in a mesh: sp: 16 (over z, x), tp: 8 (over y, core).
Axes of the slice: x: 4, y: 4, z: 4, core: 2. Of those that a mesh axis runs over, the one named last changes fastest.
Arguments:
- queries: bfloat16 [8192, 2048], P('sp', 'tp'), may hold values from -6 to 6
- keys: bfloat16 [8192, 1024], P('sp', 'tp'), may hold values from -6 to 6
- values: bfloat16 [8192, 1024], P('sp', 'tp'), may hold values from -6 to 6
- documents: int32 [8192], P('sp'), may hold values from 0 to 3, never falling along the last dimension, each value on 1 to 4096 neighbouring positions
- query_gain: float32 [128], replicated, may hold values from 1.8 to 6
- key_gain: float32 [128], replicated, may hold values from 1.8 to 6
- residual: bfloat16 [8192, 4096], P('sp', 'tp'), may hold values from -6 to 6
- out_weight: bfloat16 [2048, 4096], P('tp'), may hold values from -0.125 to 0.125
- norm_gain: float32 [4096], replicated, may hold values from 0.1 to 1.9
- up_weight: bfloat16 [4096, 16384], P('sp', 'tp'), may hold values from -0.09375 to 0.09375
- down_weight: bfloat16 [16384, 4096], P('tp', 'sp'), may hold values from -0.046875 to 0.046875
Outputs:
- mixed: bfloat16 [8192, 4096], P('sp', 'tp')
Inputs may be any that keep to these rules, and one draw needn't show every extreme that they name: `documents`: document numbers never fall along the sequence; a document has at most 4096 positions.
All inputs are finite; a program needn't handle non-finite values.
Results may differ from a plain program's by a relative error of at most 0.017.
The roundings to bfloat16 on the way count: a program that leaves them out, or rounds other values in their place, can miss the bound.
Values may be sent and summed in bfloat16 or wider, within the bound.
A program may use at most 192 MiB of HBM per device.

v0:
```python
import jax
import jax.numpy as jnp
from jax import lax
from jax.sharding import Mesh
from jax.sharding import PartitionSpec as P

D = 4096
HQ = 16
KV = 8
HD = 128
GRID_W = 64
TP = ("tp_0", "tp_1")
norm_eps = 1e-06
rope_base = 10000.0
masked_score = -1e30


def gather_turned(arrays, axis, dims):
    turned = [jnp.moveaxis(a, dim, 0) for a, dim in zip(arrays, dims)]
    both = jnp.concatenate([t.reshape(len(t), -1) for t in turned], axis=1)
    filled, at, finished = (lax.all_gather(both, axis, axis=0, tiled=True), 0, [])
    for t, dim in zip(turned, dims):
        section = filled[:, at : at + t[0].size].reshape(-1, *t.shape[1:])
        finished.append(jnp.moveaxis(section, 0, dim))
        at += t[0].size
    return tuple(finished)


def in_one_piece(arrays, axis, dim, along):
    columns = [a.reshape(*a.shape[:along], -1) for a in arrays]
    both = jnp.concatenate(columns, axis=along)
    filled, at, finished = (lax.all_gather(both, axis, axis=dim, tiled=True), 0, [])
    for a, column in zip(arrays, columns):
        section = filled[..., at : at + column.shape[along]]
        finished.append(section.reshape(*section.shape[:along], *a.shape[along:]))
        at += column.shape[along]
    return tuple(finished)


def split_up(x, dim, size):
    dims = x.shape
    pieces = x.reshape(*dims[:dim], size, dims[dim] // size, *dims[dim + 1 :])
    return jnp.moveaxis(pieces, dim, 0)


def sum_at_owner(x, axis, dim):
    pieces = split_up(x, dim, lax.axis_size(axis))
    arrived = lax.all_to_all(pieces, axis, split_axis=0, concat_axis=0, tiled=True)
    return arrived.astype(jnp.float32).sum(axis=0)


def sent_to_all(x, axis):
    copies = jnp.broadcast_to(x, (lax.axis_size(axis), *x.shape))
    return lax.all_to_all(copies, axis, split_axis=0, concat_axis=0, tiled=True)


def over_copies(x, axis):
    return sent_to_all(x, axis).sum(axis=0)


def joined_along(pieces, dim):
    pieces = jnp.moveaxis(pieces, 0, dim)
    dims = pieces.shape
    return pieces.reshape(*dims[:dim], dims[dim] * dims[dim + 1], *dims[dim + 2 :])


def whole_of(x, axes, dim):
    far, near = axes
    initial = sent_to_all(x, far)
    pieces = jnp.swapaxes(sent_to_all(initial, near), 0, 1)
    return joined_along(pieces.reshape(-1, *x.shape), dim)


def head_norm(heads_in, gain):
    values32 = heads_in.astype(jnp.float32)
    scaled = values32 * lax.rsqrt(jnp.mean(values32 * values32, axis=-1, keepdims=True) + norm_eps)
    return scaled * gain


def rotate_half(heads_in, position):
    quarter = heads_in.shape[-1] // 2
    inverse_freq = rope_base ** (-jnp.arange(quarter, dtype=jnp.float32) / quarter)
    angles = position[:, None] * inverse_freq[None, :]
    cosine_part = jnp.cos(angles)[:, None, :]
    sine_part = jnp.sin(angles)[:, None, :]
    leading = heads_in[..., :quarter]
    trailing = heads_in[..., quarter:]
    return jnp.concatenate(
        [
            leading * cosine_part - trailing * sine_part,
            leading * sine_part + trailing * cosine_part,
        ],
        axis=-1,
    )


def grid_rotary(heads_in, positions):
    half_width = heads_in.shape[-1] // 2
    grid_row = (positions // GRID_W).astype(jnp.float32)
    grid_col = (positions % GRID_W).astype(jnp.float32)
    return jnp.concatenate(
        [
            rotate_half(heads_in[..., :half_width], grid_row),
            rotate_half(heads_in[..., half_width:], grid_col),
        ],
        axis=-1,
    )


def body(
    queries,
    keys,
    values,
    documents,
    query_gain,
    key_gain,
    residual,
    out_weight,
    norm_gain,
    up_weight,
    down_weight,
):
    tok_rows = queries.shape[0]
    key_heads = keys.shape[1] // HD
    group_size = HQ // KV
    width_local = residual.shape[1]
    tp_index = lax.axis_index(TP)
    up_whole, down_whole = gather_turned((up_weight, down_weight), "sp", (0, 1))
    positions = lax.axis_index("sp") * tok_rows + jnp.arange(tok_rows, dtype=jnp.int32)
    queries_rot = grid_rotary(
        head_norm(queries.reshape(tok_rows, key_heads * group_size, HD), query_gain), positions
    )
    queries_rot = queries_rot.astype(jnp.bfloat16).reshape(tok_rows, key_heads, group_size, HD)
    keys_rot = grid_rotary(
        head_norm(keys.reshape(tok_rows, key_heads, HD), key_gain), positions
    ).astype(jnp.bfloat16)
    value_heads = values.reshape(tok_rows, key_heads, HD)
    own_docs = documents.astype(jnp.bfloat16)
    score_scale = HD ** (-0.5)
    running_max = jnp.full((key_heads, group_size, tok_rows), masked_score, jnp.float32)
    key_piece, value_piece, doc_piece = in_one_piece((keys_rot, value_heads, own_docs), "sp", 0, 1)
    scores = (
        jnp.einsum("qkgd,skd->kgqs", queries_rot, key_piece, preferred_element_type=jnp.float32)
        * score_scale
    )
    same_doc = own_docs[:, None] == doc_piece[None, :]
    scores = jnp.where(same_doc, scores, masked_score)
    new_max = jnp.maximum(running_max, jnp.max(scores, axis=-1))
    probs = jnp.where(same_doc, jnp.exp(scores - new_max[..., None]), 0.0)
    running_sum = jnp.sum(probs, axis=-1)
    update = jnp.einsum(
        "kgqs,skd->qkgd",
        probs.astype(jnp.bfloat16),
        value_piece,
        preferred_element_type=jnp.float32,
    )
    weighted = update
    running_max, running_sum, weighted = (new_max, running_sum, weighted)
    attended = (weighted / jnp.transpose(running_sum, (2, 0, 1))[..., None]).astype(jnp.bfloat16)
    attended = attended.reshape(tok_rows, key_heads * group_size * HD)
    partial_out = jnp.dot(attended, out_weight, preferred_element_type=jnp.float32)
    branch = sum_at_owner(partial_out.astype(jnp.bfloat16), TP, 1)
    stream = residual.astype(jnp.float32) + branch
    square_sum = over_copies(jnp.sum(stream * stream, axis=-1), TP)
    gain_local = lax.dynamic_slice_in_dim(norm_gain, tp_index * width_local, width_local, 0)
    normed_local = stream * lax.rsqrt(square_sum[:, None] / D + norm_eps) * gain_local
    normed = whole_of(normed_local.astype(jnp.bfloat16), ("tp_0", "tp_1"), 1)
    hidden = jnp.dot(normed, up_whole, preferred_element_type=jnp.float32)
    positive = jnp.maximum(hidden, 0.0)
    squared = (positive * positive).astype(jnp.bfloat16)
    product = jnp.dot(squared, down_whole, preferred_element_type=jnp.float32)
    feed = lax.psum_scatter(
        product.astype(jnp.bfloat16), TP, scatter_dimension=1, tiled=True
    ).astype(jnp.float32)
    return (stream + feed).astype(jnp.bfloat16)


def solution(mesh):
    split = Mesh(mesh.devices.reshape(mesh.shape["sp"], 4, 2), ("sp", "tp_0", "tp_1"))
    return jax.shard_map(
        body,
        mesh=split,
        in_specs=(
            P("sp", TP),
            P("sp", TP),
            P("sp", TP),
            P("sp"),
            P(),
            P(),
            P("sp", TP),
            P(TP, None),
            P(),
            P("sp", TP),
            P(TP, "sp"),
        ),
        out_specs=P("sp", TP),
        check_vma=False,
    )
```

profile of v0, /device:TPU:0, one launch (start us, length us, event | category | flops | bytes accessed | tf_op | source)
XLA Modules:
  0.0 357.3 jit_solution(17306286537889101392)
XLA Ops:
  6.6 1.2 copy.50
  7.8 0.7 fusion.31
  8.6 0.6 fusion.57
  9.1 0.1 copy.51
  9.3 0.1 copy.52
  9.4 0.1 copy.53
  9.5 0.1 copy.54
  9.7 0.7 convert_element_type.70
  10.3 0.1 reshape.364
  10.5 1.8 concatenate.30
  12.3 0.0 all-gather.3.cloned.1.call-update
  12.4 0.0 all-gather.5.cloned.1.call-start
  12.4 1.5 copy.64
  13.9 2.7 pad_maximum_fusion
  16.6 0.1 copy.56
  16.8 0.1 copy.57
  16.9 0.1 multiply_reduce_fusion.1
  17.0 1.9 multiply_cosine_fusion.1
  18.9 0.2 multiply_multiply_fusion
  19.1 0.5 subtract_convert_fusion.1
  19.6 56.8 %all-gather.3.cloned.1.call-done = bf16[8192,257]{1,0:T(8,128)(2,1)} async-done(((bf16[512,257]{1,0:T(8,128)(2,1)}), bf16[8192,257]{1,0:T(8,128)(2,1)}) %all-gather.3.cloned.1.call-update) | async-done | bytes 4210704 | tf_op jit(solution)/shard_map/all_gather | solution.py:32
  76.4 2.2 slice_reduce_fusion
  78.7 4.0 %broadcast_compare_fusion = pred[512,8192]{0,1:T(8,128)(4,1)} fusion(bf16[512]{0:T(512)(128)(2,1)S(1)} %convert_element_type.70, bf16[8192]{0:T(1024)(128)(2,1)S(1)} %slice_reduce_fusion), kind=kLoop, calls=%fused_computation.17 | loop fusion | flops 4194304 | bytes 4211712 | tf_op jit(solution)/shard_map/eq | solution.py:146
  82.6 17.1 %fusion = (f32[2,512]{1,0:T(2,128)S(1)}, f32[8192,512,2]{1,0,2:T(8,128)}) fusion(pred[512,8192]{0,1:T(8,128)(4,1)} %broadcast_compare_fusion, bf16[512,2,32]{2,0,1:T(8,128)(2,1)S(1)} %get-tuple-element.9, bf16[512,2,32]{2,0,1:T(8,128)(2,1)S(1)} %get-tuple-element.10, bf16[512,2,32]{2,0,1:T(8,128)(2,1)S(1)} %get-tuple-element.6, ...), kind=kOutput, calls=%fused_computation.2 | convolution fusion | flops 2173697024 | bytes 40112128 | tf_op jit(solution)/shard_map/qkgd,skd->kgqs/dot_general | solution.py:143
  99.7 15.8 %fusion.1 = f32[2,512]{1,0:T(2,128)S(1)} fusion(f32[8192,512,2]{1,0,2:T(8,128)} %get-tuple-element.24, f32[2,512]{1,0:T(2,128)S(1)} %broadcast_maximum_fusion, pred[512,8192]{0,1:T(8,128)(4,1)} %broadcast_compare_fusion), kind=kLoop, calls=%fused_computation.3 | loop fusion | flops 41942016 | bytes 37756928 | tf_op jit(solution)/shard_map/reduce_sum | solution.py:150
  115.6 17.6 %fusion.26 = bf16[512,1,2,128]{0,3,2,1:T(8,128)(2,1)S(1)} fusion(f32[8192,512,2]{1,0,2:T(8,128)} %get-tuple-element.24, f32[2,512]{1,0:T(2,128)S(1)} %broadcast_maximum_fusion, pred[512,8192]{0,1:T(8,128)(4,1)} %broadcast_compare_fusion, bf16[8192,257]{1,0:T(8,128)(2,1)} %all-gather.3.cloned.1.call-done, f32[512,2]{0,1:T(2,128)S(1)} %bitcast.100), kind=kOutput, calls=%fused_computation.30 | convolution fusion | flops 2189688832 | bytes 40116224 | tf_op jit(solution)/shard_map/kgqs,skd->qkgd/dot_general | solution.py:151
  133.1 1.3 convolution_convert_fusion
  134.4 0.4 copy.71
  134.8 53.9 %all_to_all.21 = bf16[8,512,512]{2,1,0:T(8,128)(2,1)S(1)} all-to-all(bf16[8,512,512]{2,1,0:T(8,128)(2,1)S(1)} %bitcast.94), channel_id=1, replica_groups=mesh['sp'=16,'tp_0'=4,'tp_1'=2] {'tp_0','tp_1'}, dimensions={0} | all-to-all | bytes 8388608 | tf_op jit(solution)/shard_map/all_to_all | solution.py:48
  188.8 0.6 convert_reduce_fusion
  189.4 0.2 multiply_reduce_fusion
  189.6 0.6 broadcast_in_dim.22
  190.2 3.3 all-to-all-start.1
  193.6 0.0 reduce-scatter.2.cloned.1.call-start
  193.6 0.8 dynamic_slice.3
  194.4 4.5 %all-to-all-done.1 = f32[8,1,512]{2,1,0:T(1,128)S(1)} async-done(((f32[8,1,512]{2,1,0:T(1,128)}), f32[8,1,512]{2,1,0:T(1,128)S(1)}, u32[]{:S(2)}, u32[]{:S(2)}) %all-to-all-start.1) | async-done | bytes 16416 | tf_op jit(solution)/shard_map/all_to_all | solution.py:54
  198.9 0.2 multiply_convert_fusion.1
  199.1 0.2 broadcast_in_dim.23
  199.2 29.1 %all_to_all.22 = bf16[4,512,512]{2,1,0:T(8,128)(2,1)S(1)} all-to-all(bf16[4,512,512]{2,1,0:T(8,128)(2,1)S(1)} %broadcast_in_dim.23), channel_id=1, replica_groups=mesh['sp'=16,'tp_0'=4,'tp_1'=2] {'tp_0'}, dimensions={0} | all-to-all | bytes 4194304 | tf_op jit(solution)/shard_map/all_to_all | solution.py:54
  228.4 0.4 broadcast_in_dim.26
  228.7 7.1 %all_to_all.23 = bf16[2,4,512,512]{3,2,1,0:T(8,128)(2,1)S(1)} all-to-all(bf16[2,4,512,512]{3,2,1,0:T(8,128)(2,1)S(1)} %broadcast_in_dim.26), channel_id=1, replica_groups=mesh['sp'=16,'tp_0'=4,'tp_1'=2] {'tp_1'}, dimensions={0} | all-to-all | bytes 8388608 | tf_op jit(solution)/shard_map/all_to_all | solution.py:54
  235.8 2.4 copy.62
  238.2 6.5 %copy.63 = bf16[512,8,512]{0,2,1:T(8,128)(2,1)} copy(bf16[512,8,512]{2,0,1:T(8,128)(2,1)} %bitcast.95) | data formatting | bytes 8388608 | tf_op jit(solution)/shard_map/transpose | solution.py:62
  244.8 38.8 %all-gather.5.cloned.1.call-done = bf16[4096,4096]{0,1:T(8,128)(2,1)} async-done(((bf16[256,4096]{0,1:T(8,128)(2,1)}), bf16[4096,4096]{0,1:T(8,128)(2,1)}) %all-gather.5.cloned.1.call-update) | async-done | bytes 33554448 | tf_op jit(solution)/shard_map/all_gather | solution.py:21
  283.6 13.7 %multiply_convert_fusion.clone.5 = bf16[512,2048]{1,0:T(8,128)(2,1)S(1)} fusion(bf16[512,4096]{0,1:T(8,128)(2,1)} %bitcast.96, bf16[4096,4096]{0,1:T(8,128)(2,1)} %all-gather.5.cloned.1.call-done), kind=kOutput, calls=%fused_computation.16.clone.clone.clone.2 | convolution fusion | flops 8593080320 | bytes 23068672 | tf_op jit(solution)/shard_map/dot_general | solution.py:168
  297.3 13.9 %fusion.11 = bf16[512,4096]{1,0:T(8,128)(2,1)} fusion(bf16[4096,4096]{0,1:T(8,128)(2,1)} %all-gather.5.cloned.1.call-done, bf16[512,2048]{1,0:T(8,128)(2,1)S(1)} %multiply_convert_fusion.clone.5), kind=kOutput, calls=%fused_computation.13 | convolution fusion | flops 8592031744 | bytes 23068672 | tf_op jit(solution)/shard_map/dot_general | solution.py:171
  311.3 37.3 %reduce-scatter.2.cloned.1.call-done = bf16[512,512]{1,0:T(8,128)(2,1)} async-done(((bf16[512,4096]{1,0:T(8,128)(2,1)}), bf16[512,512]{1,0:T(8,128)(2,1)}) %reduce-scatter.2.cloned.1.call-update) | async-done | bytes 524304 | tf_op jit(solution)/shard_map/reduce_scatter | solution.py:172
  348.6 2.2 add_convert_fusion
  (21 shorter events, 0.2 us)
Async XLA Ops:
  6.5 126.6 %copy-start = (bf16[256,4096]{1,0:T(8,128)(2,1)S(1)}, bf16[256,4096]{1,0:T(8,128)(2,1)}, u32[]{:S(2)}) copy-start(bf16[256,4096]{1,0:T(8,128)(2,1)} %param.18) | copy-start | bytes 6291460
  6.5 10.1 %copy-start.3 = (bf16[512,256]{1,0:T(8,128)(2,1)S(1)}, bf16[512,256]{1,0:T(8,128)(2,1)}, u32[]{:S(2)}) copy-start(bf16[512,256]{1,0:T(8,128)(2,1)} %param.11) | copy-start | bytes 786436
  6.5 69.9 %all-gather.3.cloned.1.call-start = ((), (), s32[]{:S(2)}) async-start(), calls=%async_computation.5 | async-start | bytes 6684672 | tf_op jit(solution)/shard_map/all_gather | solution.py:32
  10.5 8.4 %copy-start.4 = (f32[128]{0:T(128)S(1)}, f32[128]{0:T(128)}, u32[]{:S(2)}) copy-start(f32[128]{0:T(128)} %param.15) | copy-start | bytes 1540
  12.4 271.2 %all-gather.5.cloned.1.call-start = ((), (), s32[]{:S(2)}) async-start(), calls=%async_computation.6 | async-start | bytes 35651584 | tf_op jit(solution)/shard_map/all_gather | solution.py:21
  134.8 54.5 %copy-start.2 = (bf16[512,512]{1,0:T(8,128)(2,1)S(1)}, bf16[512,512]{1,0:T(8,128)(2,1)}, u32[]{:S(2)}) copy-start(bf16[512,512]{1,0:T(8,128)(2,1)} %param.17) | copy-start | bytes 1572868
  190.2 8.6 %all-to-all-start.1 = ((f32[8,1,512]{2,1,0:T(1,128)}), f32[8,1,512]{2,1,0:T(1,128)S(1)}, u32[]{:S(2)}, u32[]{:S(2)}) async-start(f32[8,1,512]{2,1,0:T(1,128)} %broadcast_in_dim.22), calls=%async_computation.1 | async-start | bytes 32768 | tf_op jit(solution)/shard_map/all_to_all | solution.py:54
  193.6 155.0 %reduce-scatter.2.cloned.1.call-start = ((), (), s32[]{:S(2)}) async-start(), calls=%async_computation.7 | async-start | bytes 4718592 | tf_op jit(solution)/shard_map/reduce_scatter | solution.py:172
  297.3 53.5 %copy-start.1 = (bf16[256,4096]{1,0:T(8,128)(2,1)S(1)}, bf16[256,4096]{1,0:T(8,128)(2,1)}, u32[]{:S(2)}) copy-start(bf16[256,4096]{1,0:T(8,128)(2,1)} %param.18) | copy-start | bytes 6291460
Sparse Core Ops, SparseCore 0:
  12.5 63.8 all-gather.2
  78.5 204.9 all-gather.4
  311.4 37.1 reduce-scatter.1
where the time goes:
time: 358 us; the launch traced here: 357 us
  waiting for transfers between devices  137 us (38%)
  blocking collectives  90.2 us (25%)
  matrix products  63.6 us (18%)
  other arithmetic  30.5 us (9%)
  local copies, waits for them, and re-layouts  18.9 us (5%)
  between operations  13.3 us (4%)
    all_gather x1, waiting for transfers between devices, in_one_piece(): lax.all_gather(both, axis, axis=dim, tiled=True)  56.8 us
    all_to_all x1, blocking collectives, sum_at_owner(): lax.all_to_all(pieces, axis, split_axis=0, concat_axis=0, tiled=True)  53.9 us
    all_gather x1, waiting for transfers between devices, gather_turned(): lax.all_gather(both, axis, axis=0, tiled=True)  38.8 us
    reduce_scatter x1, waiting for transfers between devices, body(): lax.psum_scatter(product.astype(jnp.bfloat16), TP, scatter_dimension=1, t...  37.3 us
    all_to_all x2, blocking collectives, sent_to_all(): return lax.all_to_all(copies, axis, split_axis=0, concat_axis=0, tiled=True)  36.2 us
    dot_general x1, matrix products, body(): jnp.einsum('kgqs,skd->qkgd', probs.astype(jnp.bfloat16), value_piece, pre...  17.6 us
    dot_general x1, matrix products, body(): jnp.einsum('qkgd,skd->kgqs', queries_rot, key_piece, preferred_element_ty...  17.1 us
    reduce_sum x1, other arithmetic, body(): running_sum = jnp.sum(probs, axis=-1)  15.8 us
  transfers between devices with their start and end apart: 4, of which 4 were waited for; matrix products, arithmetic and copies ran while one was open for 22% of the time, Pallas kernels for 0%

commit v1 on v0

--- a/solution.py
+++ b/solution.py
@@ -18,7 +18,13 @@
 def gather_turned(arrays, axis, dims):
     turned = [jnp.moveaxis(a, dim, 0) for a, dim in zip(arrays, dims)]
     both = jnp.concatenate([t.reshape(len(t), -1) for t in turned], axis=1)
-    filled, at, finished = (lax.all_gather(both, axis, axis=0, tiled=True), 0, [])
+    filled, at, finished = (
+        jnp.concatenate(
+            lax.all_to_all(jnp.stack([both] * lax.axis_size(axis)), axis, 0, 0), axis=0
+        ),
+        0,
+        [],
+    )
     for t, dim in zip(turned, dims):
         section = filled[:, at : at + t[0].size].reshape(-1, *t.shape[1:])
         finished.append(jnp.moveaxis(section, 0, dim))

time: 358 us -> 829 us (2.32)
  waiting for transfers between devices: 137 us -> 607 us
  blocking collectives: 90.2 us -> 62.2 us
  local copies, waits for them, and re-layouts: 18.9 us -> 38.9 us
  starting transfers between devices: 3.42 us -> 12.9 us
    all_to_all x0 -> x1, waiting for transfers between devices: none -> 494 us  [gather_turned(): lax.all_to_all(jnp.stack([both] * lax.axis_size(axis)), axis, 0, 0)]
    all_gather x1 -> x0, waiting for transfers between devices: 38.8 us -> none  [gather_turned(): lax.all_gather(both, axis, axis=0, tiled=True)]
    all_to_all x2 -> x1, blocking collectives: 36.2 us -> 8.28 us  [sent_to_all(): return lax.all_to_all(copies, axis, split_axis=0, concat_axis=0, tiled=True)]
    all_to_all x1 -> x2, waiting for transfers between devices: 4.45 us -> 21.7 us  [sent_to_all(): return lax.all_to_all(copies, axis, split_axis=0, concat_axis=0, tiled=True)]
    another operation x0 -> x1, local copies, waits for them, and re-layouts: none -> 10.9 us  [gather_turned(): jnp.stack([both] * lax.axis_size(axis))]
  transfers between devices with their start and end apart: 4 -> 5, of which waited for: 4 -> 5; matrix products, arithmetic and copies ran while one was open for 22% -> 3% of each run, Pallas kernels for 0% -> 0%
where the time goes in v1:
time: 829 us
  waiting for transfers between devices  607 us (73%)
  blocking collectives  62.2 us (8%)
  matrix products  61.6 us (7%)
  local copies, waits for them, and re-layouts  38.9 us (5%)
  other arithmetic  32 us (4%)
  between operations  13.6 us (2%)
  starting transfers between devices  12.9 us (2%)
    all_to_all x1, waiting for transfers between devices, gather_turned(): lax.all_to_all(jnp.stack([both] * lax.axis_size(axis)), axis, 0, 0)  494 us
    all_gather x1, waiting for transfers between devices, in_one_piece(): lax.all_gather(both, axis, axis=dim, tiled=True)  58.8 us
    all_to_all x1, blocking collectives, sum_at_owner(): lax.all_to_all(pieces, axis, split_axis=0, concat_axis=0, tiled=True)  53.9 us
    reduce_scatter x1, waiting for transfers between devices, body(): lax.psum_scatter(product.astype(jnp.bfloat16), TP, scatter_dimension=1, t...  33.2 us
    all_to_all x2, waiting for transfers between devices, sent_to_all(): return lax.all_to_all(copies, axis, split_axis=0, concat_axis=0, tiled=True)  21.7 us
    dot_general x1, matrix products, body(): jnp.einsum('kgqs,skd->qkgd', probs.astype(jnp.bfloat16), value_piece, pre...  17 us
  transfers between devices with their start and end apart: 5, of which 5 were waited for; matrix products, arithmetic and copies ran while one was open for 3% of the time, Pallas kernels for 0%

profile of v1, /device:TPU:0, one launch (start us, length us, event | category | flops | bytes accessed | tf_op | source)
XLA Modules:
  0.0 828.5 jit_solution(275133400649175441)
XLA Ops:
  6.6 1.1 copy.55
  7.8 0.7 fusion.31
  8.5 0.6 fusion.57
  9.1 0.1 copy.56
  9.2 0.1 copy.57
  9.4 0.1 copy.58
  9.5 0.1 copy.59
  9.6 0.7 convert_element_type.70
  10.3 0.1 reshape.370
  10.4 1.8 concatenate.30
  12.3 1.1 copy.61
  13.4 0.1 copy.62
  13.6 1.9 multiply_cosine_fusion.1
  15.5 0.9 multiply_multiply_fusion
  16.4 1.2 subtract_convert_fusion.1
  17.5 58.8 %all-gather.2.cloned.1.call-done = bf16[8192,257]{1,0:T(8,128)(2,1)} async-done(((bf16[512,257]{1,0:T(8,128)(2,1)}), bf16[8192,257]{1,0:T(8,128)(2,1)}) %all-gather.2.cloned.1.call-update) | async-done | bytes 4210704 | tf_op jit(solution)/shard_map/all_gather | solution.py:38
  76.4 2.2 slice_reduce_fusion
  78.6 4.0 broadcast_compare_fusion
  82.7 15.7 %fusion = (f32[2,512]{1,0:T(2,128)S(1)}, f32[8192,512,2]{1,0,2:T(8,128)}) fusion(pred[512,8192]{0,1:T(8,128)(4,1)} %broadcast_compare_fusion, bf16[512,2,32]{2,0,1:T(8,128)(2,1)S(1)} %get-tuple-element.9, bf16[512,2,32]{2,0,1:T(8,128)(2,1)S(1)} %copy-done.4, bf16[512,2,32]{2,0,1:T(8,128)(2,1)S(1)} %get-tuple-element.6, ...), kind=kOutput, calls=%fused_computation.2 | convolution fusion | flops 2173697024 | bytes 40112128 | tf_op jit(solution)/shard_map/qkgd,skd->kgqs/dot_general | solution.py:149
  98.4 15.6 %fusion.1 = f32[2,512]{1,0:T(2,128)S(1)} fusion(f32[8192,512,2]{1,0,2:T(8,128)} %get-tuple-element.24, f32[2,512]{1,0:T(2,128)S(1)} %broadcast_maximum_fusion, pred[512,8192]{0,1:T(8,128)(4,1)} %broadcast_compare_fusion), kind=kLoop, calls=%fused_computation.3 | loop fusion | flops 41942016 | bytes 37756928 | tf_op jit(solution)/shard_map/reduce_sum | solution.py:156
  114.0 17.0 %fusion.26 = bf16[512,1,2,128]{0,3,2,1:T(8,128)(2,1)S(1)} fusion(f32[8192,512,2]{1,0,2:T(8,128)} %get-tuple-element.24, f32[2,512]{1,0:T(2,128)S(1)} %broadcast_maximum_fusion, pred[512,8192]{0,1:T(8,128)(4,1)} %broadcast_compare_fusion, bf16[8192,257]{1,0:T(8,128)(2,1)} %all-gather.2.cloned.1.call-done, f32[512,2]{0,1:T(2,128)S(1)} %bitcast.101), kind=kOutput, calls=%fused_computation.30 | convolution fusion | flops 2189688832 | bytes 40116224 | tf_op jit(solution)/shard_map/kgqs,skd->qkgd/dot_general | solution.py:157
  130.9 1.3 convolution_convert_fusion
  132.2 0.4 copy.77
  132.6 53.9 %all_to_all.26 = bf16[8,512,512]{2,1,0:T(8,128)(2,1)S(1)} all-to-all(bf16[8,512,512]{2,1,0:T(8,128)(2,1)S(1)} %bitcast.95), channel_id=1, replica_groups=mesh['sp'=16,'tp_0'=4,'tp_1'=2] {'tp_0','tp_1'}, dimensions={0} | all-to-all | bytes 8388608 | tf_op jit(solution)/shard_map/all_to_all | solution.py:54
  186.6 0.6 convert_reduce_fusion
  187.2 0.2 multiply_reduce_fusion
  187.4 0.6 broadcast_in_dim.22
  188.0 3.3 all-to-all-start.1
  191.3 0.8 dynamic_slice.3
  192.1 4.5 all-to-all-done.1
  196.7 0.2 multiply_convert_fusion.1
  196.8 1.5 broadcast_in_dim.23
  198.4 3.6 all-to-all-start.2
  202.0 2.3 copy.69
  204.3 3.0 pad_maximum_fusion
  207.3 4.1 copy.70
  211.4 17.1 %all-to-all-done.2 = bf16[4,512,512]{2,1,0:T(8,128)(2,1)S(1)} async-done(((bf16[4,512,512]{2,1,0:T(8,128)(2,1)}), bf16[4,512,512]{2,1,0:T(8,128)(2,1)S(1)}, u32[]{:S(2)}, u32[]{:S(2)}) %all-to-all-start.2) | async-done | bytes 2097184 | tf_op jit(solution)/shard_map/all_to_all | solution.py:60
  228.5 0.4 broadcast_in_dim.26
  228.9 8.3 all_to_all.27
  237.2 10.9 %stack.2 = bf16[16,256,4096]{2,1,0:T(8,128)(2,1)} broadcast(bf16[256,4096]{1,0:T(8,128)(2,1)S(1)} %copy-done.2), dimensions={1,2} | broadcast | bytes 35651584 | tf_op jit(solution)/shard_map/stack | solution.py:23
  248.1 6.0 all-to-all-start.4
  254.1 4.4 copy.67
  258.5 6.5 copy.68
  264.9 493.6 %all-to-all-done.4 = bf16[16,256,4096]{2,1,0:T(8,128)(2,1)} async-done(((bf16[16,256,4096]{2,1,0:T(8,128)(2,1)}), bf16[16,256,4096]{2,1,0:T(8,128)(2,1)}, u32[]{:S(2)}, u32[]{:S(2)}) %all-to-all-start.4) | async-done | bytes 33554464 | tf_op jit(solution)/shard_map/all_to_all | solution.py:23
  758.6 13.6 %multiply_convert_fusion.clone.5 = bf16[512,2048]{1,0:T(8,128)(2,1)S(1)} fusion(bf16[512,4096]{0,1:T(8,128)(2,1)} %bitcast.97, bf16[4096,4096]{1,0:T(8,128)(2,1)} %bitcast.24), kind=kOutput, calls=%fused_computation.16.clone.clone.clone.2 | convolution fusion | flops 8593080320 | bytes 23068672 | tf_op jit(solution)/shard_map/dot_general | solution.py:174
  772.2 14.0 %fusion.11 = bf16[512,4096]{1,0:T(8,128)(2,1)} fusion(bf16[4096,4096]{1,0:T(8,128)(2,1)} %bitcast.24, bf16[512,2048]{1,0:T(8,128)(2,1)S(1)} %multiply_convert_fusion.clone.5), kind=kOutput, calls=%fused_computation.13 | convolution fusion | flops 8592031744 | bytes 23068672 | tf_op jit(solution)/shard_map/dot_general | solution.py:177
  786.3 33.2 %reduce-scatter.2.cloned.1.call-done = bf16[512,512]{1,0:T(8,128)(2,1)} async-done(((bf16[512,4096]{1,0:T(8,128)(2,1)}), bf16[512,512]{1,0:T(8,128)(2,1)}) %reduce-scatter.2.cloned.1.call-update) | async-done | bytes 524304 | tf_op jit(solution)/shard_map/reduce_scatter | solution.py:178
  819.5 2.2 add_convert_fusion
  (23 shorter events, 0.3 us)
Async XLA Ops:
  6.5 124.4 %copy-start = (bf16[256,4096]{1,0:T(8,128)(2,1)S(1)}, bf16[256,4096]{1,0:T(8,128)(2,1)}, u32[]{:S(2)}) copy-start(bf16[256,4096]{1,0:T(8,128)(2,1)} %param.18) | copy-start | bytes 6291460
  6.5 69.8 %all-gather.2.cloned.1.call-start = ((), (), s32[]{:S(2)}) async-start(), calls=%async_computation.6 | async-start | bytes 6684672 | tf_op jit(solution)/shard_map/all_gather | solution.py:38
  17.5 65.1 %copy-start.4 = (bf16[512,2,32]{2,0,1:T(8,128)(2,1)S(1)}, bf16[512,2,32]{2,0,1:T(8,128)(2,1)}, u32[]{:S(2)}) copy-start(bf16[512,2,32]{2,0,1:T(8,128)(2,1)} %get-tuple-element.10) | copy-start | bytes 196612
  132.6 54.5 %copy-start.3 = (bf16[512,512]{1,0:T(8,128)(2,1)S(1)}, bf16[512,512]{1,0:T(8,128)(2,1)}, u32[]{:S(2)}) copy-start(bf16[512,512]{1,0:T(8,128)(2,1)} %param.17) | copy-start | bytes 1572868
  188.0 8.6 %all-to-all-start.1 = ((f32[8,1,512]{2,1,0:T(1,128)}), f32[8,1,512]{2,1,0:T(1,128)S(1)}, u32[]{:S(2)}, u32[]{:S(2)}) async-start(f32[8,1,512]{2,1,0:T(1,128)} %broadcast_in_dim.22), calls=%async_computation.1 | async-start | bytes 32768 | tf_op jit(solution)/shard_map/all_to_all | solution.py:60
  198.4 30.2 %all-to-all-start.2 = ((bf16[4,512,512]{2,1,0:T(8,128)(2,1)}), bf16[4,512,512]{2,1,0:T(8,128)(2,1)S(1)}, u32[]{:S(2)}, u32[]{:S(2)}) async-start(bf16[4,512,512]{2,1,0:T(8,128)(2,1)} %broadcast_in_dim.23), calls=%async_computation.2 | async-start | bytes 4194304 | tf_op jit(solution)/shard_map/all_to_all | solution.py:60
  228.5 8.7 %copy-start.2 = (bf16[256,4096]{1,0:T(8,128)(2,1)S(1)}, bf16[256,4096]{1,0:T(8,128)(2,1)}, u32[]{:S(2)}) copy-start(bf16[256,4096]{1,0:T(8,128)(2,1)} %copy.70) | copy-start | bytes 6291460
  248.1 510.5 %all-to-all-start.4 = ((bf16[16,256,4096]{2,1,0:T(8,128)(2,1)}), bf16[16,256,4096]{2,1,0:T(8,128)(2,1)}, u32[]{:S(2)}, u32[]{:S(2)}) async-start(bf16[16,256,4096]{2,1,0:T(8,128)(2,1)} %stack.2), calls=%async_computation.4 | async-start | bytes 67108864 | tf_op jit(solution)/shard_map/all_to_all | solution.py:23
  254.0 565.4 %reduce-scatter.2.cloned.1.call-start = ((), (), s32[]{:S(2)}) async-start(), calls=%async_computation.7 | async-start | bytes 4718592 | tf_op jit(solution)/shard_map/reduce_scatter | solution.py:178
  772.2 49.5 %copy-start.1 = (bf16[256,4096]{1,0:T(8,128)(2,1)S(1)}, bf16[256,4096]{1,0:T(8,128)(2,1)}, u32[]{:S(2)}) copy-start(bf16[256,4096]{1,0:T(8,128)(2,1)} %param.18) | copy-start | bytes 6291460
Sparse Core Ops, SparseCore 0:
  12.4 63.8 all-gather.1
  786.4 33.0 reduce-scatter.1
